TPU v7x, 128 devices: a whole 4x4x4 slice. The times are simulated.
128 devices in a mesh: fs: 16 (over z, x), rep: 4 (over y), tp: 2 (over core).
Axes of the slice: x: 4, y: 4, z: 4, core: 2. Of those that a mesh axis runs over, the one named last changes fastest.
Arguments:
- saved_query: bfloat16 [196608, 512], P(('fs', 'rep')), may hold values from -30 to 30
- upstream_query: bfloat16 [196608, 1536], P(('fs', 'rep'), 'tp'), may hold values from -0.067658235 to 0.067658235
- weight_query: float32 [512, 1536], P('fs', 'tp'), may hold values from -0.25 to 0.25
- moment_query: float32 [512, 1536], P('fs', 'tp'), may hold values from -12 to 12
- left_query: bfloat16 [512, 512], P('fs'), may hold values from -2 to 2
- right_query: bfloat16 [4, 384, 384], P('tp'), may hold values from -2 to 2
- saved_output: bfloat16 [196608, 1024], P(('fs', 'rep')), may hold values from -30 to 30
- upstream_output: bfloat16 [196608, 2048], P(('fs', 'rep'), 'tp'), may hold values from -0.067658235 to 0.067658235
- weight_output: float32 [1024, 2048], P('fs', 'tp'), may hold values from -0.1875 to 0.1875
- moment_output: float32 [1024, 2048], P('fs', 'tp'), may hold values from -12 to 12
- left_output: bfloat16 [1024, 1024], P('fs'), may hold values from -2 to 2
- right_output: bfloat16 [4, 512, 512], P('tp'), may hold values from -2 to 2
Outputs:
- new_weight_query: float32 [512, 1536], P('fs', 'tp')
- new_moment_query: float32 [512, 1536], P('fs', 'tp')
- copy_query: bfloat16 [512, 1536], P(None, 'tp')
- new_weight_output: float32 [1024, 2048], P('fs', 'tp')
- new_moment_output: float32 [1024, 2048], P('fs', 'tp')
- copy_output: bfloat16 [1024, 2048], P(None, 'tp')
All inputs are finite; a program needn't handle non-finite values.
Results may differ from a plain program's by a relative error of at most 0.0085.
Values may be sent and summed in bfloat16 or wider, within the bound.
A program may use at most 128 MiB of HBM per device.

v0:
```python
import jax
import jax.numpy as jnp
from jax import lax
from jax.sharding import PartitionSpec as P


def cut_along(array, dim, peers):
    lengths = array.shape
    blocks = array.reshape(*lengths[:dim], peers, lengths[dim] // peers, *lengths[dim + 1 :])
    return jnp.moveaxis(blocks, dim, 0)


def sent_and_summed(array, axis, dim):
    blocks = cut_along(array, dim, lax.axis_size(axis))
    arrived = lax.all_to_all(blocks, axis, split_axis=0, concat_axis=0, tiled=True)
    return arrived.astype(jnp.float32).sum(axis=0)


def copy_for_each(array, axis):
    copies = jnp.broadcast_to(array, (lax.axis_size(axis), *array.shape))
    return lax.all_to_all(copies, axis, split_axis=0, concat_axis=0, tiled=True)


def over_copies(array, axis):
    return copy_for_each(array, axis).sum(axis=0)


def in_order(blocks, dim):
    lengths = list(blocks.shape[1:])
    lengths[dim] *= blocks.shape[0]
    return jnp.moveaxis(blocks, 0, dim).reshape(lengths)


def gather_directly(array, axis, dim):
    blocks = copy_for_each(array, axis)
    return in_order(blocks, dim)


def token_term(saved, upstream):

    def term(start, count):
        return lax.dot_general(
            saved, upstream, (((0,), (0,)), ((), ())), preferred_element_type=jnp.float32
        )

    return term


def left_term(left, piece):
    return jnp.dot(left, piece, preferred_element_type=jnp.float32)


def precondition(saved, upstream, left, right):
    term = token_term(saved, upstream)
    grad = sent_and_summed(
        term(jnp.int32(0), saved.shape[1] // lax.axis_size("fs") * lax.axis_size("fs")).astype(
            jnp.bfloat16
        ),
        "fs",
        0,
    )
    grad = over_copies(grad, "rep")
    rounded = grad.astype(jnp.bfloat16)
    left_prod = left_term(left, gather_directly(rounded, "fs", 0))
    left_prod = left_prod.astype(jnp.bfloat16)
    rows = left_prod.shape[0]
    block = right.shape[1]
    shaped = left_prod.reshape(rows, -1, block)
    direction = jnp.einsum("rnb,nbc->rnc", shaped, right, preferred_element_type=jnp.float32)
    direction = direction.reshape(rows, -1)
    return (jnp.sum(grad * grad), direction)


def finish(weight, moment, direction, scale):
    new_moment = 0.8 * moment + scale * direction
    new_weight = 0.998 * weight - 0.02 * new_moment
    gathered = lax.all_gather(new_weight.astype(jnp.bfloat16), "fs", axis=0, tiled=True)
    return (new_weight, new_moment, gathered)


def local(
    saved_query,
    upstream_query,
    weight_query,
    moment_query,
    left_query,
    right_query,
    saved_output,
    upstream_output,
    weight_output,
    moment_output,
    left_output,
    right_output,
):
    grad_sq_query, dir_query = precondition(saved_query, upstream_query, left_query, right_query)
    grad_sq_output, dir_output = precondition(
        saved_output, upstream_output, left_output, right_output
    )
    dir_sq_query = jnp.sum(dir_query * dir_query)
    dir_sq_output = jnp.sum(dir_output * dir_output)
    totals = over_copies(
        jnp.stack([grad_sq_query, grad_sq_output, dir_sq_query, dir_sq_output]), ("fs", "tp")
    )
    scale_query = jnp.sqrt(totals[0] / (totals[2] + 1e-06))
    scale_output = jnp.sqrt(totals[1] / (totals[3] + 1e-06))
    wq, mq, cq = finish(weight_query, moment_query, dir_query, scale_query)
    wo, mo, co = finish(weight_output, moment_output, dir_output, scale_output)
    return (wq, mq, cq, wo, mo, co)


def solution(mesh):
    return jax.shard_map(
        local,
        mesh=mesh,
        in_specs=(
            P(("fs", "rep"), None),
            P(("fs", "rep"), "tp"),
            P("fs", "tp"),
            P("fs", "tp"),
            P("fs", None),
            P("tp", None, None),
            P(("fs", "rep"), None),
            P(("fs", "rep"), "tp"),
            P("fs", "tp"),
            P("fs", "tp"),
            P("fs", None),
            P("tp", None, None),
        ),
        out_specs=(
            P("fs", "tp"),
            P("fs", "tp"),
            P(None, "tp"),
            P("fs", "tp"),
            P("fs", "tp"),
            P(None, "tp"),
        ),
        check_vma=False,
    )
```

profile of v0, /device:TPU:0, one launch (start us, length us, event | category | flops | bytes accessed | tf_op | source)
XLA Modules:
  0.0 230.3 jit_solution(9761300126585062830)
XLA Ops:
  9.1 5.9 %convolution_convert_fusion.1 = bf16[512,768]{1,0:T(8,128)(2,1)} fusion(bf16[3072,512]{1,0:T(8,128)(2,1)S(1)} %copy-done, bf16[3072,768]{1,0:T(8,128)(2,1)} %param.13), kind=kOutput, calls=%fused_computation.3 | convolution fusion | flops 2416312320 | bytes 8650752 | tf_op jit(solution)/shard_map/dot_general | solution.py:42
  14.9 8.0 %all-to-all-start = ((bf16[16,32,768]{2,1,0:T(8,128)(2,1)}), bf16[16,32,768]{2,1,0:T(8,128)(2,1)}, u32[]{:S(2)}, u32[]{:S(2)}) async-start(bf16[16,32,768]{2,1,0:T(8,128)(2,1)} %bitcast.44), calls=%async_computation | async-start | bytes 1572864 | tf_op jit(solution)/shard_map/all_to_all | solution.py:15
  23.0 11.6 %convolution_convert_fusion = bf16[1024,1024]{1,0:T(8,128)(2,1)} fusion(bf16[3072,1024]{1,0:T(8,128)(2,1)} %param.18, bf16[3072,1024]{1,0:T(8,128)(2,1)} %param.19), kind=kOutput, calls=%fused_computation.1 | convolution fusion | flops 6443499520 | bytes 14680064 | tf_op jit(solution)/shard_map/dot_general | solution.py:42
  34.6 2.9 %all-to-all-done = bf16[16,32,768]{2,1,0:T(8,128)(2,1)} async-done(((bf16[16,32,768]{2,1,0:T(8,128)(2,1)}), bf16[16,32,768]{2,1,0:T(8,128)(2,1)}, u32[]{:S(2)}, u32[]{:S(2)}) %all-to-all-start) | async-done | bytes 786464 | tf_op jit(solution)/shard_map/all_to_all | solution.py:15
  37.5 4.4 %all-to-all-start.2 = ((bf16[16,64,1024]{2,1,0:T(8,128)(2,1)}), bf16[16,64,1024]{2,1,0:T(8,128)(2,1)}, u32[]{:S(2)}, u32[]{:S(2)}) async-start(bf16[16,64,1024]{2,1,0:T(8,128)(2,1)} %bitcast.42), calls=%async_computation.2 | async-start | bytes 4194304 | tf_op jit(solution)/shard_map/all_to_all | solution.py:15
  43.2 29.0 %all-to-all-done.2 = bf16[16,64,1024]{2,1,0:T(8,128)(2,1)} async-done(((bf16[16,64,1024]{2,1,0:T(8,128)(2,1)}), bf16[16,64,1024]{2,1,0:T(8,128)(2,1)}, u32[]{:S(2)}, u32[]{:S(2)}) %all-to-all-start.2) | async-done | bytes 2097184 | tf_op jit(solution)/shard_map/all_to_all | solution.py:15
  73.0 4.5 %all-to-all-start.1 = ((f32[4,32,768]{2,1,0:T(8,128)}), f32[4,32,768]{2,1,0:T(8,128)S(1)}, u32[]{:S(2)}, u32[]{:S(2)}) async-start(f32[4,32,768]{2,1,0:T(8,128)} %broadcast_in_dim.15), calls=%async_computation.1 | async-start | bytes 786432 | tf_op jit(solution)/shard_map/all_to_all | solution.py:21
  77.4 2.7 %convert_reduce_fusion = f32[64,1024]{1,0:T(8,128)} fusion(bf16[16,64,1024]{2,1,0:T(8,128)(2,1)} %all-to-all-done.2), kind=kLoop, calls=%fused_computation | loop fusion | flops 2031616 | bytes 2359296 | tf_op jit(solution)/shard_map/reduce_sum | solution.py:16
  80.1 4.7 %all-to-all-done.1 = f32[4,32,768]{2,1,0:T(8,128)S(1)} async-done(((f32[4,32,768]{2,1,0:T(8,128)}), f32[4,32,768]{2,1,0:T(8,128)S(1)}, u32[]{:S(2)}, u32[]{:S(2)}) %all-to-all-start.1) | async-done | bytes 393248 | tf_op jit(solution)/shard_map/all_to_all | solution.py:21
  84.8 2.0 broadcast_in_dim.16
  86.9 4.2 %all-to-all-start.3 = ((f32[4,64,1024]{2,1,0:T(8,128)}), f32[4,64,1024]{2,1,0:T(8,128)}, u32[]{:S(2)}, u32[]{:S(2)}) async-start(f32[4,64,1024]{2,1,0:T(8,128)} %broadcast_in_dim.16), calls=%async_computation.3 | async-start | bytes 2097152 | tf_op jit(solution)/shard_map/all_to_all | solution.py:21
  93.4 9.3 %all-to-all-done.3 = f32[4,64,1024]{2,1,0:T(8,128)} async-done(((f32[4,64,1024]{2,1,0:T(8,128)}), f32[4,64,1024]{2,1,0:T(8,128)}, u32[]{:S(2)}, u32[]{:S(2)}) %all-to-all-start.3) | async-done | bytes 1048608 | tf_op jit(solution)/shard_map/all_to_all | solution.py:21
  103.6 6.7 %all-to-all-start.4 = ((bf16[16,32,768]{2,1,0:T(8,128)(2,1)}), bf16[16,32,768]{2,1,0:T(8,128)(2,1)}, u32[]{:S(2)}, u32[]{:S(2)}) async-start(bf16[16,32,768]{2,1,0:T(8,128)(2,1)} %broadcast_in_dim.17), calls=%async_computation.4 | async-start | bytes 1572864 | tf_op jit(solution)/shard_map/all_to_all | solution.py:21
  112.3 10.4 %all-to-all-done.4 = bf16[16,32,768]{2,1,0:T(8,128)(2,1)} async-done(((bf16[16,32,768]{2,1,0:T(8,128)(2,1)}), bf16[16,32,768]{2,1,0:T(8,128)(2,1)}, u32[]{:S(2)}, u32[]{:S(2)}) %all-to-all-start.4) | async-done | bytes 786464 | tf_op jit(solution)/shard_map/all_to_all | solution.py:21
  124.2 4.6 %all-to-all-start.5 = ((bf16[16,64,1024]{2,1,0:T(8,128)(2,1)}), bf16[16,64,1024]{2,1,0:T(8,128)(2,1)}, u32[]{:S(2)}, u32[]{:S(2)}) async-start(bf16[16,64,1024]{2,1,0:T(8,128)(2,1)} %broadcast_in_dim.18), calls=%async_computation.5 | async-start | bytes 4194304 | tf_op jit(solution)/shard_map/all_to_all | solution.py:21
  132.1 24.0 %all-to-all-done.5 = bf16[16,64,1024]{2,1,0:T(8,128)(2,1)} async-done(((bf16[16,64,1024]{2,1,0:T(8,128)(2,1)}), bf16[16,64,1024]{2,1,0:T(8,128)(2,1)}, u32[]{:S(2)}, u32[]{:S(2)}) %all-to-all-start.5) | async-done | bytes 2097184 | tf_op jit(solution)/shard_map/all_to_all | solution.py:21
  156.2 2.1 convolution_convert_fusion.2
  158.2 2.1 multiply_reduce_fusion
  160.4 2.7 %pad_maximum_fusion = f32[4]{0:T(128)S(1)} fusion(f32[1]{0:T(128)} %bitcast.9, f32[1]{0:T(128)} %bitcast.6, f32[1]{0:T(128)} %bitcast.3, f32[1]{0:T(128)} %bitcast.1), kind=kLoop, calls=%fused_computation.22 | loop fusion | flops 12 | bytes 32 | tf_op jit(solution)/shard_map/stack | solution.py:102
  163.1 10.3 %all_to_all.36 = f32[32,1,4]{2,1,0:T(1,128)S(1)} all-to-all(f32[32,1,4]{2,1,0:T(1,128)S(1)} %broadcast_in_dim.19), channel_id=1, replica_groups=mesh['fs'=16,'rep'=4,'tp'=2] {'fs','tp'}, dimensions={0} | all-to-all | bytes 1024 | tf_op jit(solution)/shard_map/all_to_all | solution.py:21
  180.4 24.7 %all_gather.6 = bf16[512,768]{1,0:T(8,128)(2,1)} all-gather(bf16[32,768]{1,0:T(8,128)(2,1)S(1)} %get-tuple-element.9), channel_id=1, replica_groups=mesh['fs'=16,'rep'=4,'tp'=2] {'fs'}, dimensions={0}, use_global_device_ids=true | all-gather | bytes 835584 | tf_op jit(solution)/shard_map/all_gather | solution.py:77
  205.1 13.2 %all-gather.2.cloned.1.call-done = bf16[1024,1024]{1,0:T(8,128)(2,1)} async-done(((bf16[64,1024]{1,0:T(8,128)(2,1)}), bf16[1024,1024]{1,0:T(8,128)(2,1)}) %all-gather.2.cloned.1.call-update) | async-done | bytes 2097168 | tf_op jit(solution)/shard_map/all_gather | solution.py:77
  218.3 2.1 copy.56
  220.4 3.1 %copy.57 = bf16[1024,1024]{1,0:T(8,128)(2,1)} copy(bf16[1024,1024]{1,0:T(8,128)(2,1)} %all-gather.2.cloned.1.call-done) | data formatting | bytes 4194304
  (27 shorter events, 18.3 us)
Async XLA Ops:
  7.2 1.9 copy-start
  14.9 22.6 %all-to-all-start = ((bf16[16,32,768]{2,1,0:T(8,128)(2,1)}), bf16[16,32,768]{2,1,0:T(8,128)(2,1)}, u32[]{:S(2)}, u32[]{:S(2)}) async-start(bf16[16,32,768]{2,1,0:T(8,128)(2,1)} %bitcast.44), calls=%async_computation | async-start | bytes 1572864 | tf_op jit(solution)/shard_map/all_to_all | solution.py:15
  37.5 34.7 %all-to-all-start.2 = ((bf16[16,64,1024]{2,1,0:T(8,128)(2,1)}), bf16[16,64,1024]{2,1,0:T(8,128)(2,1)}, u32[]{:S(2)}, u32[]{:S(2)}) async-start(bf16[16,64,1024]{2,1,0:T(8,128)(2,1)} %bitcast.42), calls=%async_computation.2 | async-start | bytes 4194304 | tf_op jit(solution)/shard_map/all_to_all | solution.py:15
  73.0 11.8 %all-to-all-start.1 = ((f32[4,32,768]{2,1,0:T(8,128)}), f32[4,32,768]{2,1,0:T(8,128)S(1)}, u32[]{:S(2)}, u32[]{:S(2)}) async-start(f32[4,32,768]{2,1,0:T(8,128)} %broadcast_in_dim.15), calls=%async_computation.1 | async-start | bytes 786432 | tf_op jit(solution)/shard_map/all_to_all | solution.py:21
  86.9 15.8 %all-to-all-start.3 = ((f32[4,64,1024]{2,1,0:T(8,128)}), f32[4,64,1024]{2,1,0:T(8,128)}, u32[]{:S(2)}, u32[]{:S(2)}) async-start(f32[4,64,1024]{2,1,0:T(8,128)} %broadcast_in_dim.16), calls=%async_computation.3 | async-start | bytes 2097152 | tf_op jit(solution)/shard_map/all_to_all | solution.py:21
  103.6 19.0 %all-to-all-start.4 = ((bf16[16,32,768]{2,1,0:T(8,128)(2,1)}), bf16[16,32,768]{2,1,0:T(8,128)(2,1)}, u32[]{:S(2)}, u32[]{:S(2)}) async-start(bf16[16,32,768]{2,1,0:T(8,128)(2,1)} %broadcast_in_dim.17), calls=%async_computation.4 | async-start | bytes 1572864 | tf_op jit(solution)/shard_map/all_to_all | solution.py:21
  122.7 6.2 %copy-start.2 = (bf16[32,512]{1,0:T(8,128)(2,1)S(1)}, bf16[32,512]{1,0:T(8,128)(2,1)}, u32[]{:S(2)}) copy-start(bf16[32,512]{1,0:T(8,128)(2,1)} %param.16) | copy-start | bytes 98308
  124.2 31.9 %copy-start.1 = (bf16[64,1024]{1,0:T(8,128)(2,1)S(1)}, bf16[64,1024]{1,0:T(8,128)(2,1)}, u32[]{:S(2)}) copy-start(bf16[64,1024]{1,0:T(8,128)(2,1)} %param.22) | copy-start | bytes 393220
  124.2 31.9 %all-to-all-start.5 = ((bf16[16,64,1024]{2,1,0:T(8,128)(2,1)}), bf16[16,64,1024]{2,1,0:T(8,128)(2,1)}, u32[]{:S(2)}, u32[]{:S(2)}) async-start(bf16[16,64,1024]{2,1,0:T(8,128)(2,1)} %broadcast_in_dim.18), calls=%async_computation.5 | async-start | bytes 4194304 | tf_op jit(solution)/shard_map/all_to_all | solution.py:21
  128.8 89.5 %all-gather.2.cloned.1.call-start = ((), (), s32[]{:S(2)}) async-start(), calls=%async_computation.7 | async-start | bytes 2228224 | tf_op jit(solution)/shard_map/all_gather | solution.py:77
Sparse Core Ops, SparseCore 0:
  177.5 40.7 all-gather.1
where the time goes:
time: 232 us; the launch traced here: 230 us
  waiting for transfers between devices  93.5 us (40%)
  blocking collectives  35.1 us (15%)
  starting transfers between devices  32.4 us (14%)
  matrix products  25 us (11%)
  between operations  16.8 us (7%)
  other arithmetic  14.5 us (6%)
  local copies, waits for them, and re-layouts  13 us (6%)
    all_to_all x4, waiting for transfers between devices, copy_for_each(): return lax.all_to_all(copies, axis, split_axis=0, concat_axis=0, tiled=True)  48.4 us
    all_to_all x2, waiting for transfers between devices, sent_and_summed(): lax.all_to_all(blocks, axis, split_axis=0, concat_axis=0, tiled=True)  31.9 us
    all_gather x1, blocking collectives, finish(): lax.all_gather(new_weight.astype(jnp.bfloat16), 'fs', axis=0, tiled=True)  24.7 us
    all_to_all x4, starting transfers between devices, copy_for_each(): return lax.all_to_all(copies, axis, split_axis=0, concat_axis=0, tiled=True)  19.9 us
    dot_general x2, matrix products, term(): lax.dot_general(saved, upstream, (((0,), (0,)), ((), ())), preferred_elem...  17.5 us
    all_gather x1, waiting for transfers between devices, finish(): lax.all_gather(new_weight.astype(jnp.bfloat16), 'fs', axis=0, tiled=True)  13.2 us
    all_to_all x2, starting transfers between devices, sent_and_summed(): lax.all_to_all(blocks, axis, split_axis=0, concat_axis=0, tiled=True)  12.5 us
    all_to_all x1, blocking collectives, copy_for_each(): return lax.all_to_all(copies, axis, split_axis=0, concat_axis=0, tiled=True)  10.3 us
  transfers between devices with their start and end apart: 7, of which 7 were waited for; matrix products, arithmetic and copies ran while one was open for 11% of the time, Pallas kernels for 0%

commit v1 on v0

v1 whole, which is shorter than its diff:
```python
import functools

import jax
import jax.numpy as jnp
from jax import lax
from jax.experimental import pallas as pl
from jax.experimental.pallas import tpu as pltpu
from jax.sharding import PartitionSpec as P

MESH = pl.DeviceIdType.MESH
BF = jnp.bfloat16
F32 = jnp.float32
HBM = pl.BlockSpec(memory_space=pl.ANY)

TOK = 3072
STREAMS = {"q": (16, 16, 16), "a": (16, 32, 16), "b": (16, 16, 32)}
ORDER = ("xyz", "yzx", "zxy")


def vmem_scratch():
    s = {}
    s["uq"] = ((TOK, 768), BF)
    s["sq"] = ((TOK, 512), BF)
    s["uo"] = ((TOK, 1024), BF)
    s["so"] = ((TOK, 1024), BF)
    s["rq"] = ((2, 384, 384), BF)
    s["ro"] = ((2, 512, 512), BF)
    s["wq"] = ((32, 768), F32)
    s["mq"] = ((32, 768), F32)
    s["wo"] = ((64, 1024), F32)
    s["mo"] = ((64, 1024), F32)
    s["lq"] = ((4, 32, 512), BF)
    s["lo"] = ((4, 64, 1024), BF)
    for c, rows in STREAMS.items():
        for t, nr in enumerate(rows):
            s[f"a1{c}{t}"] = ((4, 16 * nr, 128), BF)
            s[f"r1{c}{t}"] = ((3, 16 * nr, 128), BF)
            s[f"a2{c}{t}"] = ((4, 4 * nr, 128), BF)
            s[f"r2{c}{t}"] = ((3, 4 * nr, 128), BF)
            s[f"a3{c}{t}"] = ((4, nr, 128), BF)
            s[f"r3{c}{t}"] = ((3, nr, 128), BF)
    s["gq"] = ((4, 48, 128), BF)
    s["go"] = ((2, 4, 64, 128), BF)
    s["psq"] = ((64, 128), BF)
    s["pq"] = ((16, 64, 128), BF)
    s["pso"] = ((4, 48, 128), BF)
    s["po"] = ((16, 48, 128), BF)
    s["dq"] = ((128, 768), F32)
    s["do"] = ((64, 1024), F32)
    for c in "qo":
        s[f"cs{c}"] = ((16, 128), F32)
        s[f"cr{c}"] = ((16, 128), F32)
        s[f"ps{c}2"] = ((8, 128), F32)
        s[f"pr{c}2"] = ((16, 8, 128), F32)
    s["cq"] = ((4, 4, 32, 768), BF)
    s["co"] = ((4, 4, 64, 1024), BF)
    return s


SCRATCH = vmem_scratch()


class Sems:
    def __init__(self, ref):
        self.ref = ref
        self.n = 0

    def new(self):
        self.n += 1
        return self.ref.at[self.n - 1]


N_SEMS = 200


def kernel(*refs):
    names = [
        f"{n}_{k}" for k in "qo" for n in ("saved", "up", "weight", "moment", "left", "right")
    ]
    i = dict(zip(names, refs[:12]))
    o_wq, o_mq, o_cq, o_wo, o_mo, o_co = refs[12:18]
    v = dict(zip(SCRATCH, refs[18 : 18 + len(SCRATCH)]))
    sems = Sems(refs[18 + len(SCRATCH)])

    fs = lax.axis_index("fs")
    y = lax.axis_index("rep")
    c = lax.axis_index("tp")
    z = lax.div(fs, 4)
    x = lax.rem(fs, 4)
    me = {"x": x, "y": y, "z": z}

    def off(d, k):
        return lax.rem(me[d] + k, 4)

    def dev(dz=0, dx=0, dy=0, dc=0):
        return (
            lax.rem(z + dz, 4) * 4 + lax.rem(x + dx, 4),
            lax.rem(y + dy, 4),
            lax.rem(c + dc, 2),
        )

    def along(d, k):
        return dev(**{"d" + d: k})

    sent = []

    def local(src, dst):
        sem = sems.new()
        cp = pltpu.make_async_copy(src, dst, sem)
        cp.start()
        return cp

    def send(src, dst, ss, rs, to):
        pltpu.make_async_remote_copy(
            src_ref=src, dst_ref=dst, send_sem=ss, recv_sem=rs, device_id=to, device_id_type=MESH
        ).start()

    def wait(ref, sem):
        pltpu.make_async_copy(ref, ref, sem).wait()

    ld = {}
    ld["uq"] = local(i["up_q"], v["uq"])
    ld["sq"] = local(i["saved_q"], v["sq"])
    ld["lo"] = local(i["left_o"], v["lo"].at[x])
    ld["lq"] = local(i["left_q"], v["lq"].at[x])
    for h in range(2):
        for k in range(4):
            ld[f"so{h}{k}"] = local(
                i["saved_o"].at[:, pl.ds((k * 2 + h) * 128, 128)],
                v["so"].at[:, pl.ds((h * 4 + k) * 128, 128)],
            )
        if h == 0:
            ld["uo"] = local(i["up_o"], v["uo"])
    ld["rq"] = local(i["right_q"], v["rq"])
    ld["ro"] = local(i["right_o"], v["ro"])
    for n, k in (("weight_q", "wq"), ("moment_q", "mq"), ("weight_o", "wo"), ("moment_o", "mo")):
        ld[k] = local(i[n], v[k])

    peers = [dict(dc=1)]
    peers += [dict(dx=a, dy=b) for a in range(4) for b in range(4) if a or b]
    peers += [dict(dz=a, dx=b) for a in range(1, 4) for b in range(4)]
    barrier = pltpu.get_barrier_semaphore()
    for p in peers:
        pl.semaphore_signal(barrier, inc=1, device_id=dev(**p), device_id_type=MESH)
    pl.semaphore_wait(barrier, len(peers))

    def left_start(k, half):
        ld[k].wait()
        ss, rs = sems.new(), sems.new()
        part = v[k].at[x, pl.ds(c * half, half)]
        for d in (1, 2, 3):
            send(part, part, ss, rs, along("x", d))
        sent.append((v[k].at[pl.ds(0, 3), pl.ds(0, half)], ss))
        return rs

    lsem = {"lo": left_start("lo", 32), "lq": left_start("lq", 16)}

    def left_forward(k, half):
        wait(v[k].at[pl.ds(0, 3), pl.ds(0, half)], lsem[k])
        ss, rs = sems.new(), sems.new()
        for d in (1, 2, 3):
            part = v[k].at[off("x", d), pl.ds(c * half, half)]
            send(part, part, ss, rs, dev(dc=1))
        sent.append((v[k].at[pl.ds(0, 3), pl.ds(0, half)], ss))
        lsem[k] = rs

    def left_done(k, half):
        wait(v[k].at[pl.ds(0, 3), pl.ds(0, half)], lsem[k])

    def grad(chunk, saved, upstream, lane0, half):
        rows = upstream.shape[1] // 2
        r = rows // 8
        res = lax.dot_general(
            upstream[:, half * rows : (half + 1) * rows],
            saved[:, lane0 : lane0 + 512],
            (((0,), (0,)), ((), ())),
            preferred_element_type=F32,
        ).astype(BF)
        for xl in range(2):
            for yy in range(4):
                for zz in range(4):
                    at = {"x": half * 2 + xl, "y": yy, "z": zz}
                    r0 = (xl * 4 + yy) * r
                    for t, nr in enumerate(STREAMS[chunk]):
                        d1, d2, d3 = (at[d] for d in ORDER[t])
                        v[f"a1{chunk}{t}"][d1, pl.ds((d2 * 4 + d3) * nr, nr), :] = res[
                            r0 : r0 + nr, zz * 128 : zz * 128 + 128
                        ]
                        r0 += nr

    rsem = {}

    def rs_start(chunk, phase):
        for t in range(3):
            a, b = v[f"a{phase}{chunk}{t}"], v[f"r{phase}{chunk}{t}"]
            d = ORDER[t][phase - 1]
            ss, rs = sems.new(), sems.new()
            for k in (2, 1, 3):
                send(a.at[off(d, k)], b.at[k - 1], ss, rs, along(d, k))
            sent.append((b, ss))
            rsem[phase, chunk, t] = rs

    def rs_sum(chunk, phase, t):
        a, b = v[f"a{phase}{chunk}{t}"], v[f"r{phase}{chunk}{t}"]
        wait(b, rsem[phase, chunk, t])
        own = me[ORDER[t][phase - 1]]
        return (
            a[own].astype(F32) + b[0].astype(F32) + b[1].astype(F32) + b[2].astype(F32)
        ).astype(BF)

    def rs_next(chunk, phase):
        for t, nr in enumerate(STREAMS[chunk]):
            total = rs_sum(chunk, phase, t)
            dst = v[f"a{phase + 1}{chunk}{t}"]
            dst[...] = total.reshape(dst.shape)
        rs_start(chunk, phase + 1)

    gsem = {}

    def rs_end(chunk, g):
        r0 = 0
        for t, nr in enumerate(STREAMS[chunk]):
            g[z, pl.ds(r0, nr), :] = rs_sum(chunk, 3, t)
            r0 += nr
        ss, rs = sems.new(), sems.new()
        for k in (2, 1, 3):
            send(g.at[z], g.at[z], ss, rs, along("z", k))
        sent.append((g.at[pl.ds(0, 3)], ss))
        gsem[chunk] = rs

    def square_rows(total):
        hi = total.astype(BF).astype(F32)
        mid = (total - hi).astype(BF).astype(F32)
        low = total - hi - mid
        lane = lax.broadcasted_iota(jnp.int32, (16, 128), 1)
        row = lax.broadcasted_iota(jnp.int32, (16, 128), 0)
        out = jnp.where(lane == 0, hi, jnp.where(lane == 1, mid, jnp.where(lane == 2, low, 0.0)))
        return jnp.where(row == 0, out, 0.0).astype(BF)

    def total_of(a):
        return jnp.sum(jnp.sum(a, axis=1, keepdims=True), axis=0, keepdims=True)

    psem = {}

    def plane_send(k, src_of, dst):
        ss, rs = sems.new(), sems.new()
        for a in (2, 1, 3, 0):
            for b in (2, 1, 3, 0):
                if a or b:
                    send(src_of(off("x", a)), dst.at[x * 4 + y], ss, rs, dev(dx=a, dy=b))
        sent.append((dst.at[pl.ds(0, 15)], ss))
        psem[k] = rs

    def left_q():
        wait(v["gq"].at[pl.ds(0, 3)], gsem["q"])
        left_done("lq", 16)
        g = jnp.concatenate([v["gq"][k] for k in range(4)], axis=1)
        prod = lax.dot_general(
            g, v["lq"][...].reshape(128, 512), (((1,), (1,)), ((), ())), preferred_element_type=F32
        )
        gf = g.astype(F32)
        v["psq"][pl.ds(0, 48), :] = prod.astype(BF)
        v["psq"][pl.ds(48, 16), :] = square_rows(total_of(gf * gf))
        v["pq"][x * 4 + y] = v["psq"][...]
        plane_send("q", lambda k: v["psq"], v["pq"])

    def left_o():
        for ch in range(2):
            wait(v["go"].at[ch, pl.ds(0, 3)], gsem["ab"[ch]])
        left_done("lo", 32)
        g = jnp.concatenate([v["go"][h, k] for k in range(4) for h in range(2)], axis=1)
        prod = lax.dot_general(
            v["lo"][...].reshape(256, 1024),
            g,
            (((1,), (1,)), ((), ())),
            preferred_element_type=F32,
        )
        gf = g.astype(F32)
        sq = square_rows(total_of(gf * gf))
        for k in range(4):
            both = jnp.concatenate(
                [prod[k * 64 : k * 64 + 32], prod[k * 64 + 32 : k * 64 + 64]], axis=1
            )
            v["pso"][k, pl.ds(0, 32), :] = both.astype(BF)
            v["pso"][k, pl.ds(32, 16), :] = sq
        v["po"][x * 4 + y] = v["pso"][x]
        plane_send("o", lambda k: v["pso"].at[k], v["po"])

    csem = {}

    def core_send(k, direction, gsq):
        sq = direction * direction
        n = sq.shape[0] // 8
        rows = sum(sq[j * 8 : j * 8 + 8] for j in range(n))
        tile = sum(rows[:, j * 128 : j * 128 + 128] for j in range(sq.shape[1] // 128))
        v["cs" + k][pl.ds(0, 8), :] = tile
        v["cs" + k][pl.ds(8, 8), :] = jnp.broadcast_to(gsq, (8, 128))
        ss, rs = sems.new(), sems.new()
        send(v["cs" + k], v["cr" + k], ss, rs, dev(dc=1))
        sent.append((v["cr" + k], ss))
        csem[k] = rs

    def right_q():
        wait(v["pq"].at[pl.ds(0, 15)], psem["q"])
        ld["rq"].wait()
        for n in range(2):
            left = v["pq"][pl.ds(8 * n, 8), pl.ds(0, 48), :].reshape(384, 128)
            v["dq"][:, n * 384 : n * 384 + 384] = lax.dot_general(
                left, v["rq"][n], (((0,), (0,)), ((), ())), preferred_element_type=F32
            )
        gsq = total_of(sum(v["pq"][p, pl.ds(48, 16), :].astype(F32) for p in range(16)))
        core_send("q", v["dq"][pl.ds(x * 32, 32), :], gsq)

    def right_o():
        wait(v["po"].at[pl.ds(0, 15)], psem["o"])
        ld["ro"].wait()
        lane = lax.broadcasted_iota(jnp.int32, (32, 128), 1)
        top, low = [], []
        for j in range(8):
            p0 = v["po"][2 * j, pl.ds(0, 32), :].astype(F32)
            p1 = v["po"][2 * j + 1, pl.ds(0, 32), :].astype(F32)
            top.append(jnp.where(lane < 64, p0, pltpu.roll(p1, 64, 1)))
            low.append(jnp.where(lane < 64, pltpu.roll(p0, 64, 1), p1))
        for n in range(2):
            left = jnp.concatenate(
                [
                    jnp.concatenate(top[4 * n : 4 * n + 4], axis=1),
                    jnp.concatenate(low[4 * n : 4 * n + 4], axis=1),
                ],
                axis=0,
            ).astype(BF)
            v["do"][:, n * 512 : n * 512 + 512] = jnp.dot(
                left, v["ro"][n], preferred_element_type=F32
            )
        gsq = total_of(sum(v["po"][p, pl.ds(32, 16), :].astype(F32) for p in range(16)))
        core_send("o", v["do"][...], gsq)

    ssem = {}

    def sums_send(k):
        wait(v["cr" + k], csem[k])
        v[f"ps{k}2"][...] = v["cs" + k][pl.ds(0, 8), :] + v["cr" + k][pl.ds(0, 8), :]
        v[f"pr{k}2"][fs] = v[f"ps{k}2"][...]
        ss, rs = sems.new(), sems.new()
        for a in (2, 1, 3, 0):
            for b in (2, 1, 3, 0):
                if a or b:
                    send(v[f"ps{k}2"], v[f"pr{k}2"].at[fs], ss, rs, dev(dz=a, dx=b))
        sent.append((v[f"pr{k}2"].at[pl.ds(0, 15)], ss))
        ssem[k] = rs

    outs = []

    def finish(k, direction):
        wait(v[f"pr{k}2"].at[pl.ds(0, 15)], ssem[k])
        dsq = total_of(sum(v[f"pr{k}2"][p] for p in range(16)))
        gsq = v["cs" + k][pl.ds(8, 1), pl.ds(0, 1)] + v["cr" + k][pl.ds(8, 1), pl.ds(0, 1)]
        scale = jnp.sqrt(gsq / (dsq + 1e-6))
        ld["w" + k].wait()
        ld["m" + k].wait()
        moment = 0.8 * v["m" + k][...] + scale * direction
        weight = 0.998 * v["w" + k][...] - 0.02 * moment
        v["c" + k][z, x] = weight.astype(BF)
        return moment, weight

    def keep(k, moment, weight, o_m, o_w):
        v["m" + k][...] = moment
        v["w" + k][...] = weight
        outs.append(local(v["m" + k], o_m))
        outs.append(local(v["w" + k], o_w))

    class Gather:
        def __init__(self, k, n1, n2, n3):
            self.buf = v["c" + k]
            self.lanes = [pl.ds(0, n1 * 128), pl.ds(n1 * 128, n2 * 128)]
            if n3:
                self.lanes.append(pl.ds(pl.multiple_of((n1 + n2 + y) * 128, 128), 128))
            self.s = {}

        def block(self, t, dz=0, dx=0):
            return self.buf.at[off("z", dz), off("x", dx), :, self.lanes[t]]

        def push(self, t, key, blocks, d):
            ss, rs = sems.new(), sems.new()
            for b in blocks:
                for k in (2, 1, 3):
                    send(self.block(t, *b), self.block(t, *b), ss, rs, along(d, k))
            n = 3 * len(blocks)
            size = self.size(t)
            ref = (
                self.buf.at[0, pl.ds(0, 3), :, size]
                if n == 3
                else self.buf.at[pl.ds(0, 3), pl.ds(0, 3), :, size]
            )
            sent.append((ref, ss))
            self.s[t, key] = (ref, rs)

        def size(self, t):
            return pl.ds(0, 128) if t == 2 else self.lanes[t]

        def ready(self, t, key):
            wait(*self.s[t, key])

        def start(self):
            self.push(0, "x", [(0, 0)], "x")
            self.push(1, "z", [(0, 0)], "z")
            if len(self.lanes) > 2:
                self.push(2, "x", [(0, 0)], "x")
                self.push(2, "z0", [(0, 0)], "z")
            self.push(0, "z0", [(0, 0)], "z")
            self.push(1, "x0", [(0, 0)], "x")

        def second(self):
            if len(self.lanes) > 2:
                self.ready(2, "x")
                near = [(0, 2), (0, 1), (0, 3)]
                self.push(2, "z1", near, "z")
                self.push(2, "y1", near, "y")
            self.ready(0, "x")
            self.push(0, "z1", [(0, 2), (0, 1), (0, 3)], "z")
            self.ready(1, "z")
            self.push(1, "x1", [(2, 0), (1, 0), (3, 0)], "x")

        def third(self):
            if len(self.lanes) > 2:
                self.ready(2, "z0")
                self.push(2, "y2", [(2, 0), (1, 0), (3, 0)], "y")
                self.ready(2, "z1")
                for k in (1, 2, 3):
                    self.push(2, f"y3{k}", [(2, k), (1, k), (3, k)], "y")

        def end(self):
            for t, key in list(self.s):
                if (t, key) in ((0, "x"), (1, "z"), (2, "x"), (2, "z0"), (2, "z1")):
                    continue
                self.ready(t, key)

    ld["uq"].wait()
    ld["sq"].wait()
    grad("q", v["sq"], v["uq"], 0, 0)
    grad("q", v["sq"], v["uq"], 0, 1)
    rs_start("q", 1)
    for k in range(4):
        ld[f"so0{k}"].wait()
    ld["uo"].wait()
    grad("a", v["so"], v["uo"], 0, 0)
    left_forward("lo", 32)
    left_forward("lq", 16)
    grad("a", v["so"], v["uo"], 0, 1)
    rs_start("a", 1)
    for k in range(4):
        ld[f"so1{k}"].wait()
    rs_next("q", 1)
    grad("b", v["so"], v["uo"], 512, 0)
    rs_next("q", 2)
    grad("b", v["so"], v["uo"], 512, 1)
    rs_start("b", 1)
    rs_end("q", v["gq"])
    rs_next("a", 1)
    left_q()
    rs_next("a", 2)
    rs_next("b", 1)
    rs_end("a", v["go"].at[0])
    right_q()
    rs_next("b", 2)
    sums_send("q")
    rs_end("b", v["go"].at[1])
    mq, wq = finish("q", v["dq"][pl.ds(x * 32, 32), :])
    gat_q = Gather("q", 3, 3, 0)
    left_o()
    gat_q.start()
    keep("q", mq, wq, o_mq, o_wq)
    right_o()
    gat_q.second()
    sums_send("o")
    gat_q.end()
    outs.append(local(v["cq"], o_cq))
    mo, wo = finish("o", v["do"][...])
    gat_o = Gather("o", 2, 2, 4)
    gat_o.start()
    keep("o", mo, wo, o_mo, o_wo)
    gat_o.second()
    gat_o.third()
    gat_o.end()
    outs.append(local(v["co"], o_co))
    for ref, ss in sent:
        wait(ref, ss)
    for cp in outs:
        cp.wait()
    assert sems.n <= N_SEMS, sems.n


def local_fn(*args):
    shapes = [
        ((32, 768), F32),
        ((32, 768), F32),
        ((4, 4, 32, 768), BF),
        ((64, 1024), F32),
        ((64, 1024), F32),
        ((4, 4, 64, 1024), BF),
    ]
    out = pl.pallas_call(
        kernel,
        name="update",
        out_shape=[jax.ShapeDtypeStruct(s, d) for s, d in shapes],
        in_specs=[HBM] * 12,
        out_specs=[HBM] * 6,
        scratch_shapes=[pltpu.VMEM(s, d) for s, d in SCRATCH.values()]
        + [pltpu.SemaphoreType.DMA((N_SEMS,))],
        compiler_params=pltpu.CompilerParams(
            collective_id=0, has_side_effects=True, vmem_limit_bytes=60 * 1024 * 1024
        ),
    )(*args)
    wq, mq, cq, wo, mo, co = out
    return wq, mq, cq.reshape(512, 768), wo, mo, co.reshape(1024, 1024)


def solution(mesh):
    return jax.shard_map(
        local_fn,
        mesh=mesh,
        in_specs=(
            P(("fs", "rep"), None),
            P(("fs", "rep"), "tp"),
            P("fs", "tp"),
            P("fs", "tp"),
            P("fs", None),
            P("tp", None, None),
            P(("fs", "rep"), None),
            P(("fs", "rep"), "tp"),
            P("fs", "tp"),
            P("fs", "tp"),
            P("fs", None),
            P("tp", None, None),
        ),
        out_specs=(
            P("fs", "tp"),
            P("fs", "tp"),
            P(None, "tp"),
            P("fs", "tp"),
            P("fs", "tp"),
            P(None, "tp"),
        ),
        check_vma=False,
    )
```

time: 232 us -> 92.2 us (0.40)
  waiting for transfers between devices: 93.5 us -> 0 us
  Pallas kernels: 0 us -> 79.7 us
  blocking collectives: 35.1 us -> 0 us
  starting transfers between devices: 32.4 us -> 0 us
  matrix products: 25 us -> 0 us
  between operations: 16.8 us -> 0.65 us
  other arithmetic: 14.5 us -> 0 us
    all_to_all x6 -> x0, waiting for transfers between devices: 80.3 us -> none  [the longest x4 48.4 us: copy_for_each(): return lax.all_to_all(copies, axis, split_axis=0, concat_axis=0, tiled=True)]
    pallas_call x0 -> x1, Pallas kernels: none -> 79.7 us  [local_fn(): pl.pallas_call(kernel, name='update', out_shape=[jax.ShapeDtypeStruct(s,...]
    all_to_all x6 -> x0, starting transfers between devices: 32.4 us -> none  [the longest x4 19.9 us: copy_for_each(): return lax.all_to_all(copies, axis, split_axis=0, concat_axis=0, tiled=True)]
    dot_general x6 -> x0, matrix products: 25 us -> none  [the longest x2 17.5 us: term(): lax.dot_general(saved, upstream, (((0,), (0,)), ((), ())), preferred_elem...]
    all_gather x1 -> x0, blocking collectives: 24.7 us -> none  [finish(): lax.all_gather(new_weight.astype(jnp.bfloat16), 'fs', axis=0, tiled=True)]
    all_gather x1 -> x0, waiting for transfers between devices: 13.2 us -> none  [finish(): lax.all_gather(new_weight.astype(jnp.bfloat16), 'fs', axis=0, tiled=True)]
    all_to_all x1 -> x0, blocking collectives: 10.3 us -> none  [copy_for_each(): return lax.all_to_all(copies, axis, split_axis=0, concat_axis=0, tiled=True)]
    reduce_sum x7 -> x0, other arithmetic: 8.24 us -> none  [the longest x2 3.95 us: sent_and_summed(): return arrived.astype(jnp.float32).sum(axis=0)]
  transfers between devices with their start and end apart: 7 -> 0, of which waited for: 7 -> 0; matrix products, arithmetic and copies ran while one was open for 11% -> 0% of each run, Pallas kernels for 0% -> 0%
where the time goes in v1:
time: 92.2 us; the launch traced here: 91.9 us
  Pallas kernels  79.7 us (86%)
  local copies, waits for them, and re-layouts  11.6 us (13%)
    pallas_call x1, Pallas kernels, local_fn(): pl.pallas_call(kernel, name='update', out_shape=[jax.ShapeDtypeStruct(s,...  79.7 us
    unnamed x6, local copies, waits for them, and re-layouts  11.6 us

profile of v1, /device:TPU:0, one launch (start us, length us, event | category | flops | bytes accessed | tf_op | source)
XLA Modules:
  0.0 91.9 jit_solution(5180333317274937072)
XLA Ops:
  0.6 79.7 %update.1 = (f32[32,768]{1,0:T(8,128)}, f32[32,768]{1,0:T(8,128)}, bf16[4,4,32,768]{3,2,1,0:T(8,128)(2,1)}, f32[64,1024]{1,0:T(8,128)}, f32[64,1024]{1,0:T(8,128)}, /*index=5*/bf16[4,4,64,1024]{3,2,1,0:T(8,128)(2,1)}) custom-call(bf16[3072,512]{1,0:T(8,128)(2,1)} %refs_0_.1, bf16[3072,768]{1,0:T(8,128)(2,1)} %refs_1_.1, f32[32,768]{1,0:T(8,128)} %refs_2_.1, ...), custom_call_target="tpu_custom_call" | custom-call | tf_op jit(solution)/shard_map/update/pallas_call | solution.py:502
  80.3 1.5 %copy.24 = f32[32,768]{1,0:T(8,128)} copy(f32[32,768]{1,0:T(8,128)} %get-tuple-element.24) | data formatting | bytes 196608
  81.9 1.5 %copy.25 = f32[32,768]{1,0:T(8,128)} copy(f32[32,768]{1,0:T(8,128)} %get-tuple-element.25) | data formatting | bytes 196608
  83.4 2.1 %copy.26 = bf16[512,768]{1,0:T(8,128)(2,1)} copy(bf16[512,768]{1,0:T(8,128)(2,1)} %bitcast.3) | data formatting | bytes 1572864
  85.5 1.7 %copy.27 = f32[64,1024]{1,0:T(8,128)} copy(f32[64,1024]{1,0:T(8,128)} %get-tuple-element.27) | data formatting | bytes 524288
  87.1 1.7 %copy.28 = f32[64,1024]{1,0:T(8,128)} copy(f32[64,1024]{1,0:T(8,128)} %get-tuple-element.28) | data formatting | bytes 524288
  88.8 3.1 %copy.29 = bf16[1024,1024]{1,0:T(8,128)(2,1)} copy(bf16[1024,1024]{1,0:T(8,128)(2,1)} %bitcast.2) | data formatting | bytes 4194304
